TPU v7x, 32 devices: a whole 2x2x4 slice. The times are simulated.
32 devices in a mesh: sp: 4 (over y, core), dp: 8 (over z, x).
Axes of the slice: x: 2, y: 2, z: 4, core: 2. Of those that a mesh axis runs over, the one named last changes fastest.
Arguments:
- stream: bfloat16 [8, 512, 2064], P('dp', 'sp'), may hold values from -6 to 6
- mix_gain: float32 [2064], replicated, may hold values from 0.1 to 1.9
- query_weight: bfloat16 [2064, 2048], P('dp'), may hold values from -0.125 to 0.125
- query_gain: float32 [128], replicated, may hold values from 0.1 to 1.9
- keys: bfloat16 [8, 512, 512], P('dp', 'sp'), may hold values from -6 to 6
- key_gain: float32 [128], replicated, may hold values from 0.1 to 1.9
- values: bfloat16 [8, 512, 512], P('dp', 'sp'), may hold values from -48 to 48
- stick_offset: float32 [16], replicated, may hold values from -8.5 to -7, as said below
Outputs:
- attended: bfloat16 [8, 512, 2048], P('dp', 'sp')
Inputs may be any that keep to these rules, and one draw needn't show every extreme that they name: `stick_offset`: one offset for each query head, added to all of that head's scores.
All inputs are finite; a program needn't handle non-finite values.
Results may differ from a plain program's by a relative error of at most 0.012.
Values may be sent and summed in bfloat16 or wider, within the bound.
A program may use at most 64 MiB of HBM per device.

v0:
```python
import math

import jax
import jax.numpy as jnp
from jax import lax
from jax.sharding import PartitionSpec as P

norm_eps = 1e-06
row_block = 256
key_block = 128


def rms_scaled(inputs, gain):
    wide = inputs.astype(jnp.float32)
    scaled = wide * lax.rsqrt(jnp.mean(wide * wide, axis=-1, keepdims=True) + norm_eps) * gain
    return scaled.astype(jnp.bfloat16)


def stick_weights(scores, first_row):
    heads_here = scores.shape[0]
    rows_here = scores.shape[1]
    keys_here = scores.shape[2]
    width = math.gcd(keys_here, key_block)
    blocks_here = keys_here // width
    query_pos = first_row + jnp.arange(rows_here, dtype=jnp.int32)
    key_pos = jnp.arange(keys_here, dtype=jnp.int32)
    causal = key_pos[None, :] < query_pos[:, None]
    log_keep = jnp.where(causal, jax.nn.log_sigmoid(-scores), 0.0)
    pieces = log_keep.reshape(heads_here, rows_here, blocks_here, width)
    inner = jnp.arange(width, dtype=jnp.int32)
    upper = (inner[:, None] > inner[None, :]).astype(jnp.float32)
    local = jnp.einsum("hqbk,kj->hqbj", pieces, upper, precision=lax.Precision.HIGHEST)
    totals = jnp.sum(pieces, axis=3)
    later = lax.cumsum(totals, axis=2, reverse=True) - totals
    tail = (local + later[:, :, :, None]).reshape(heads_here, rows_here, keys_here)
    return jnp.where(causal, jnp.exp(jax.nn.log_sigmoid(scores) + tail), 0.0)


def body(stream, mix_gain, query_weight, query_gain, keys, key_gain, values, stick_offset):
    sp_count = lax.axis_size("sp")
    sp_index = lax.axis_index("sp")
    stream_rows = stream[0]
    tokens_dev = stream_rows.shape[0]
    head_width = query_gain.shape[0]
    heads_all = stick_offset.shape[0]
    heads_dev = heads_all // sp_count
    kv_count = keys.shape[2] // head_width
    group_size = sp_count // kv_count
    seq_length = tokens_dev * sp_count
    stacked = jnp.stack((keys[0], values[0]), axis=1).reshape(tokens_dev, 2, kv_count, head_width)
    copied = jnp.repeat(stacked, group_size, axis=2)
    arrived = lax.all_to_all(copied, "sp", split_axis=2, concat_axis=0, tiled=True)
    key_value = arrived[:, :, 0, :]
    normed = rms_scaled(stream_rows, mix_gain)
    columns = lax.dynamic_slice_in_dim(
        query_weight, sp_index * (heads_dev * head_width), heads_dev * head_width, 1
    )
    gathered = lax.all_gather(columns, "dp", axis=0, tiled=True)
    queries = jnp.dot(
        lax.all_gather(normed, "sp", axis=0, tiled=True),
        gathered,
        preferred_element_type=jnp.float32,
    ).astype(jnp.bfloat16)
    queries = lax.optimization_barrier(queries)
    mine = rms_scaled(queries.reshape(seq_length, heads_dev, head_width), query_gain)
    key_heads = rms_scaled(key_value[:, 0], key_gain)
    value_rows = key_value[:, 1]
    offsets = lax.dynamic_slice_in_dim(stick_offset, sp_index * heads_dev, heads_dev)
    block = math.gcd(seq_length, row_block)
    outputs = []
    for block_id in range(seq_length // block):
        first = block_id * block
        finish = first + block
        scores = jnp.einsum(
            "qhd,kd->hqk",
            mine[first:finish],
            key_heads[:finish],
            preferred_element_type=jnp.float32,
        )
        scores = scores * head_width ** (-0.5) + offsets[:, None, None]
        weights = stick_weights(scores, first).astype(jnp.bfloat16)
        outputs.append(
            jnp.einsum(
                "hqk,kd->qhd", weights, value_rows[:finish], preferred_element_type=jnp.float32
            )
        )
    attended = (
        jnp.concatenate(outputs, axis=0)
        .reshape(seq_length, heads_dev * head_width)
        .astype(jnp.bfloat16)
    )
    returned = lax.all_to_all(attended, "sp", split_axis=0, concat_axis=1, tiled=True)
    return returned[None]


def solution(mesh):
    return jax.shard_map(
        body,
        mesh=mesh,
        in_specs=(
            P("dp", "sp", None),
            P(),
            P("dp", None),
            P(),
            P("dp", "sp", None),
            P(),
            P("dp", "sp", None),
            P(),
        ),
        out_specs=P("dp", "sp", None),
        check_vma=False,
    )
```

profile of v0, /device:TPU:0, one launch (start us, length us, event | category | flops | bytes accessed | tf_op | source)
XLA Modules:
  0.0 124.1 jit_solution(3568556610034957392)
XLA Ops:
  6.6 1.2 copy-done
  7.8 0.7 dynamic-slice_bitcast_fusion
  8.6 1.3 %fusion.15 = f32[128]{0:T(128)S(1)} fusion(bf16[1,128,2064]{1,2,0:T(8,128)(2,1)} %param.8), kind=kLoop, calls=%fused_computation.31 | loop fusion | flops 792448 | bytes 528896 | tf_op jit(solution)/shard_map/reduce_sum | solution.py:15
  9.9 2.2 %fusion.17 = bf16[128,2064]{0,1:T(8,128)(2,1)} fusion(bf16[1,128,2064]{1,2,0:T(8,128)(2,1)} %param.8, f32[2064]{0:T(1024)} %param.9, f32[128]{0:T(128)S(1)} %add_rsqrt_fusion.2), kind=kLoop, calls=%fused_computation.33 | loop fusion | flops 1056768 | bytes 1065536 | tf_op jit(solution)/shard_map/convert_element_type | solution.py:16
  12.5 0.9 copy.56
  13.3 4.3 %all-to-all-start = ((bf16[128,2,4,128]{3,0,1,2:T(8,128)(2,1)}), bf16[128,2,4,128]{3,0,1,2:T(8,128)(2,1)S(1)}, u32[]{:S(2)}, u32[]{:S(2)}) async-start(bf16[128,2,4,128]{3,0,1,2:T(8,128)(2,1)} %copy.56), calls=%async_computation | async-start | bytes 524288 | tf_op jit(solution)/shard_map/all_to_all | solution.py:52
  17.7 0.7 iota_compare_fusion
  18.5 5.2 %all-to-all-done = bf16[128,2,4,128]{3,0,1,2:T(8,128)(2,1)S(1)} async-done(((bf16[128,2,4,128]{3,0,1,2:T(8,128)(2,1)}), bf16[128,2,4,128]{3,0,1,2:T(8,128)(2,1)S(1)}, u32[]{:S(2)}, u32[]{:S(2)}) %all-to-all-start) | async-done | bytes 262176 | tf_op jit(solution)/shard_map/all_to_all | solution.py:52
  23.8 0.8 fusion.29
  24.6 37.5 %all-gather.6.cloned.1.call-done = bf16[8,258,512]{2,1,0:T(8,128)(2,1)} async-done(((bf16[1,258,512]{2,1,0:T(8,128)(2,1)}), bf16[8,258,512]{2,1,0:T(8,128)(2,1)}) %all-gather.6.cloned.1.call-update) | async-done | bytes 2113552 | tf_op jit(solution)/shard_map/all_gather | solution.py:58
  62.1 1.9 %reshape.90 = bf16[2064,512]{1,0:T(8,128)(2,1)S(1)} reshape(bf16[8,258,512]{2,1,0:T(8,128)(2,1)} %all-gather.6.cloned.1.call-done) | data formatting | bytes 4227072
  63.9 21.1 %all-gather.4.cloned.1.call-done = bf16[512,2064]{0,1:T(8,128)(2,1)} async-done(((bf16[128,2064]{0,1:T(8,128)(2,1)}), bf16[512,2064]{0,1:T(8,128)(2,1)}) %all-gather.4.cloned.1.call-update) | async-done | bytes 2113552 | tf_op jit(solution)/shard_map/all_gather | solution.py:60
  85.1 3.8 %convolution_convert_fusion = bf16[512,512]{1,0:T(8,128)(2,1)} fusion(bf16[512,2064]{0,1:T(8,128)(2,1)} %all-gather.4.cloned.1.call-done, bf16[2064,512]{1,0:T(8,128)(2,1)S(1)} %reshape.90), kind=kOutput, calls=%fused_computation.26 | convolution fusion | flops 1082392576 | bytes 4751360 | tf_op jit(solution)/shard_map/dot_general | solution.py:59
  88.9 1.4 %reshape.88 = f32[512,4,128]{2,1,0:T(4,128)S(1)} reshape(bf16[512,512]{1,0:T(8,128)(2,1)} %convolution_convert_fusion) | data formatting | bytes 1572864 | tf_op jit(solution)/shard_map/convert_element_type | solution.py:14
  91.4 0.8 copy-done.5
  92.2 1.8 %bitcast_reduce_fusion.1 = (f32[4,256,2]{1,2,0:T(2,128)S(1)}, f32[4,256,256]{1,2,0:T(8,128)S(1)}, f32[4,256,256]{1,2,0:T(8,128)S(1)}) fusion(pred[256,256]{0,1:T(8,128)(4,1)S(1)} %iota_compare_fusion.1, f32[4]{0:T(128)S(1)} %dynamic_slice.7, bf16[512,4,128]{2,0,1:T(8,128)(2,1)S(1)} %fusion.26, bf16[512,128]{1,0:T(8,128)(2,1)} %fusion.29), kind=kOutput, calls=%fused_computation.71 | convolution fusion | flops 69990400 | bytes 2499072 | tf_op jit(solution)/shard_map/qhd,kd->hqk/dot_general | solution.py:74
  94.1 0.7 convolution_add_fusion.1
  94.8 0.8 fusion.22
  95.6 1.0 fusion.13
  96.6 3.1 %bitcast_reduce_fusion = (f32[4,256,4]{1,2,0:T(4,128)S(1)}, f32[4,256,512]{1,2,0:T(8,128)}, f32[512,256,4]{1,0,2:T(8,128)S(1)}) fusion(f32[4]{0:T(128)S(1)} %dynamic_slice.7, pred[256,512]{0,1:T(8,128)(4,1)S(1)} %copy-done.3, bf16[512,4,128]{2,0,1:T(8,128)(2,1)S(1)} %copy-done.6, bf16[512,128]{1,0:T(8,128)(2,1)S(1)} %copy-done.9), kind=kOutput, calls=%fused_computation.70 | convolution fusion | flops 139980800 | bytes 4735488 | tf_op jit(solution)/shard_map/qhd,kd->hqk/dot_general | solution.py:74
  99.7 2.9 %convolution_add_fusion = f32[4,256,4,128]{1,3,2,0:T(8,128)S(1)} fusion(f32[4,256,4,128]{1,3,2,0:T(8,128)} %bitcast.99, f32[4,256,4]{1,2,0:T(4,128)S(1)} %sub.15), kind=kOutput, calls=%fused_computation.19 | convolution fusion | flops 805847040 | bytes 4210688 | tf_op jit(solution)/shard_map/hqbk,kj->hqbj/dot_general | solution.py:32
  102.6 1.8 %fusion.4 = bf16[4,256,512]{1,2,0:T(8,128)(2,1)S(1)} fusion(f32[4,256,4,128]{1,3,2,0:T(8,128)S(1)} %convolution_add_fusion, f32[512,256,4]{1,0,2:T(8,128)S(1)} %get-tuple-element.9, f32[4]{0:T(128)S(1)} %dynamic_slice.7, pred[256,512]{0,1:T(8,128)(4,1)S(1)} %copy-done.4), kind=kLoop, calls=%fused_computation.8 | loop fusion | flops 6815744 | bytes 5373968 | tf_op jit(solution)/shard_map/convert_element_type | solution.py:81
  105.0 11.2 %all_to_all.28 = bf16[4,128,512]{1,2,0:T(8,128)(2,1)S(1)} all-to-all(bf16[4,128,512]{1,2,0:T(8,128)(2,1)S(1)} %copy.66), channel_id=1, replica_groups=mesh['sp'=4,'dp'=8] {'sp'}, dimensions={0} | all-to-all | bytes 1048576 | tf_op jit(solution)/shard_map/all_to_all | solution.py:92
  116.2 1.0 copy.67
  (50 shorter events, 2.4 us)
Async XLA Ops:
  6.5 1.2 copy-start
  6.5 5.6 %copy-start.7 = (bf16[1,128,512]{2,1,0:T(8,128)(2,1)S(1)}, bf16[1,128,512]{2,1,0:T(8,128)(2,1)}, u32[]{:S(2)}) copy-start(bf16[1,128,512]{2,1,0:T(8,128)(2,1)} %param.12) | copy-start | bytes 393220
  6.5 5.8 %copy-start.8 = (bf16[1,128,512]{2,1,0:T(8,128)(2,1)S(1)}, bf16[1,128,512]{2,1,0:T(8,128)(2,1)}, u32[]{:S(2)}) copy-start(bf16[1,128,512]{2,1,0:T(8,128)(2,1)} %param.14) | copy-start | bytes 393220
  6.5 55.5 %all-gather.6.cloned.1.call-start = ((), (), s32[]{:S(2)}) async-start(), calls=%async_computation.3 | async-start | bytes 2433024 | tf_op jit(solution)/shard_map/all_gather | solution.py:58
  8.5 9.1 %copy-start.12 = (f32[16]{0:T(128)S(1)}, f32[16]{0:T(128)}, u32[]{:S(2)}) copy-start(f32[16]{0:T(128)} %param.15) | copy-start | bytes 196
  8.5 76.5 %all-gather.4.cloned.1.call-start = ((), (), s32[]{:S(2)}) async-start(), calls=%async_computation.2 | async-start | bytes 2641920 | tf_op jit(solution)/shard_map/all_gather | solution.py:60
  9.9 13.9 %copy-start.10 = (f32[128]{0:T(128)S(1)}, f32[128]{0:T(128)}, u32[]{:S(2)}) copy-start(f32[128]{0:T(128)} %param.13) | copy-start | bytes 1540
  13.3 10.3 %all-to-all-start = ((bf16[128,2,4,128]{3,0,1,2:T(8,128)(2,1)}), bf16[128,2,4,128]{3,0,1,2:T(8,128)(2,1)S(1)}, u32[]{:S(2)}, u32[]{:S(2)}) async-start(bf16[128,2,4,128]{3,0,1,2:T(8,128)(2,1)} %copy.56), calls=%async_computation | async-start | bytes 524288 | tf_op jit(solution)/shard_map/all_to_all | solution.py:52
  88.9 2.2 %copy-start.1 = (bf16[512,512]{1,0:T(8,128)(2,1)S(1)}, bf16[512,512]{1,0:T(8,128)(2,1)}, u32[]{:S(2)}) copy-start(bf16[512,512]{1,0:T(8,128)(2,1)} %convolution_convert_fusion) | copy-start | bytes 1572868
  88.9 2.2 %copy-start.11 = (f32[128]{0:T(128)S(1)}, f32[128]{0:T(128)}, u32[]{:S(2)}) copy-start(f32[128]{0:T(128)} %param.11) | copy-start | bytes 1540
  91.4 0.8 copy-start.5
  94.7 1.8 %copy-start.3 = (pred[256,512]{0,1:T(8,128)(4,1)S(1)}, pred[256,512]{0,1:T(8,128)(4,1)}, u32[]{:S(2)}) copy-start(pred[256,512]{0,1:T(8,128)(4,1)} %iota_compare_fusion) | copy-start | bytes 393220
  94.7 1.8 %copy-start.6 = (bf16[512,4,128]{2,0,1:T(8,128)(2,1)S(1)}, bf16[512,4,128]{2,0,1:T(8,128)(2,1)}, u32[]{:S(2)}) copy-start(bf16[512,4,128]{2,0,1:T(8,128)(2,1)} %copy-done.5) | copy-start | bytes 1572868
  94.8 1.8 %copy-start.9 = (bf16[512,128]{1,0:T(8,128)(2,1)S(1)}, bf16[512,128]{1,0:T(8,128)(2,1)}, u32[]{:S(2)}) copy-start(bf16[512,128]{1,0:T(8,128)(2,1)} %fusion.29) | copy-start | bytes 393220
  99.7 2.9 %copy-start.4 = (pred[256,512]{0,1:T(8,128)(4,1)S(1)}, pred[256,512]{0,1:T(8,128)(4,1)}, u32[]{:S(2)}) copy-start(pred[256,512]{0,1:T(8,128)(4,1)} %iota_compare_fusion) | copy-start | bytes 393220
  102.6 2.1 %copy-start.2 = (bf16[256,4,128]{0,2,1:T(8,128)(2,1)S(1)}, bf16[256,4,128]{0,2,1:T(8,128)(2,1)}, u32[]{:S(2)}) copy-start(bf16[256,4,128]{0,2,1:T(8,128)(2,1)} %fusion.13) | copy-start | bytes 786436
Sparse Core Ops, SparseCore 0:
  9.5 52.5 all-gather.5
  63.6 21.4 all-gather.3
where the time goes:
time: 125 us; the launch traced here: 124 us
  waiting for transfers between devices  63.8 us (51%)
  between operations  13.7 us (11%)
  matrix products  13.5 us (11%)
  blocking collectives  11.2 us (9%)
  other arithmetic  9.01 us (7%)
  local copies, waits for them, and re-layouts  8.58 us (7%)
  starting transfers between devices  4.31 us (3%)
    all_gather x1, waiting for transfers between devices, body(): gathered = lax.all_gather(columns, 'dp', axis=0, tiled=True)  37.5 us
    all_gather x1, waiting for transfers between devices, body(): lax.all_gather(normed, 'sp', axis=0, tiled=True)  21.1 us
    all_to_all x1, blocking collectives, body(): lax.all_to_all(attended, 'sp', split_axis=0, concat_axis=1, tiled=True)  11.2 us
    all_to_all x1, waiting for transfers between devices, body(): lax.all_to_all(copied, 'sp', split_axis=2, concat_axis=0, tiled=True)  5.16 us
    unnamed x30, local copies, waits for them, and re-layouts  4.87 us
    dot_general x2, matrix products, body(): jnp.einsum('qhd,kd->hqk', mine[first:finish], key_heads[:finish], preferr...  4.85 us
    all_to_all x1, starting transfers between devices, body(): lax.all_to_all(copied, 'sp', split_axis=2, concat_axis=0, tiled=True)  4.26 us
    dot_general x1, matrix products, body(): jnp.dot(lax.all_gather(normed, 'sp', axis=0, tiled=True), gathered, prefe...  3.8 us
  transfers between devices with their start and end apart: 3, of which 3 were waited for; matrix products, arithmetic and copies ran while one was open for 7% of the time, Pallas kernels for 0%

commit v1 on v0

--- a/solution.py
+++ b/solution.py
@@ -1,13 +1,17 @@
+import functools
 import math
 
 import jax
 import jax.numpy as jnp
 from jax import lax
+from jax.experimental import pallas as pl
+from jax.experimental.pallas import tpu as pltpu
 from jax.sharding import PartitionSpec as P
 
 norm_eps = 1e-06
 row_block = 256
 key_block = 128
+MESH = pl.DeviceIdType.MESH
 
 
 def rms_scaled(inputs, gain):
@@ -36,7 +40,7 @@
     return jnp.where(causal, jnp.exp(jax.nn.log_sigmoid(scores) + tail), 0.0)
 
 
-def body(stream, mix_gain, query_weight, query_gain, keys, key_gain, values, stick_offset):
+def general_body(stream, mix_gain, query_weight, query_gain, keys, key_gain, values, stick_offset):
     sp_count = lax.axis_size("sp")
     sp_index = lax.axis_index("sp")
     stream_rows = stream[0]
@@ -93,7 +97,357 @@
     return returned[None]
 
 
+def kernel(
+    nz, nx, heads, stream, mix_gain, weight, query_gain, keys, key_gain, values, offset, out,
+    xraw, xs, wb, kraw, kn, vb, acc, ob,
+    own_sem, wrecv, wsend, xrecv, xsend, krecv, ksend, vrecv, vsend, orecv, osend,
+):
+    sp_count = xraw.shape[0]
+    tokens, width = xraw.shape[1:]
+    seq = sp_count * tokens
+    hd = query_gain.shape[1]
+    depth = wb.shape[1]
+    dp_count = nz * nx
+    dp = lax.axis_index("dp")
+    sp = lax.axis_index("sp")
+    z, x = dp // nx, lax.rem(dp, nx)
+    side = z * nx + (1 - x)
+    pair = 2 * (sp // 2) + (1 - lax.rem(sp, 2))
+    across = lax.rem(sp + 2, sp_count)
+    corner = lax.rem(pair + 2, sp_count)
+    peers = (across, pair, corner)
+    chunks = xrecv.shape[1]
+    part = tokens // chunks
+
+    barrier = pltpu.get_barrier_semaphore()
+    for peer in peers:
+        pl.semaphore_signal(barrier, inc=1, device_id={"sp": peer}, device_id_type=MESH)
+    pl.semaphore_signal(barrier, inc=1, device_id={"dp": side}, device_id_type=MESH)
+    has_up, has_down = z < nz - 1, z > 0
+
+    @pl.when(has_up)
+    def _():
+        pl.semaphore_signal(barrier, inc=1, device_id={"dp": dp + nx}, device_id_type=MESH)
+
+    @pl.when(has_down)
+    def _():
+        pl.semaphore_signal(barrier, inc=1, device_id={"dp": dp - nx}, device_id_type=MESH)
+
+    pl.semaphore_wait(barrier, 4 + jnp.where(has_up, 1, 0) + jnp.where(has_down, 1, 0))
+
+    base = sp * (heads * hd)
+    low, high = z, nz - 1 - z
+    both = jnp.minimum(low, high)
+
+    def order(i):
+        if i == 0:
+            return z
+        near = z + (i + 1) // 2 if i % 2 else z - i // 2
+        far = jnp.where(high > low, z + (i - both), z - (i - both))
+        return jnp.where(i <= 2 * both, near, far)
+
+    def w_copy(link, target, rank, h):
+        zz = order(rank)
+        block = zz * nx + x
+        if rank == 0:
+            src = weight.at[:, pl.ds(pl.multiple_of(base + h * hd, hd), hd)]
+        else:
+            src = wb.at[block, :, pl.ds(h * hd, hd)]
+        return pltpu.make_async_remote_copy(
+            src_ref=src,
+            dst_ref=wb.at[block, :, pl.ds(h * hd, hd)],
+            send_sem=wsend.at[link, rank, h],
+            recv_sem=wrecv.at[block, h],
+            device_id={"dp": target},
+            device_id_type=MESH,
+        )
+
+    def w_send(rank, h, act):
+        zz = order(rank)
+
+        @pl.when(has_up & (zz <= z))
+        def _():
+            act(w_copy(0, dp + nx, rank, h))
+
+        @pl.when(has_down & (zz >= z))
+        def _():
+            act(w_copy(1, dp - nx, rank, h))
+
+        act(w_copy(2, side, rank, h))
+
+    def w_wait(block, h):
+        ref = wb.at[block, :, pl.ds(h * hd, hd)]
+        pltpu.make_async_remote_copy(
+            src_ref=ref, dst_ref=ref, send_sem=wsend.at[0, 0, 0], recv_sem=wrecv.at[block, h],
+            device_id={"dp": side}, device_id_type=MESH,
+        ).wait_recv()
+
+    def start(copy):
+        copy.start()
+
+    def finish_send(copy):
+        copy.wait_send()
+
+    def x_copy(source, c, link, target):
+        rows = pl.ds(c * part, part)
+        src = stream.at[0, rows] if link < 2 else xraw.at[source, rows]
+        return pltpu.make_async_remote_copy(
+            src_ref=src, dst_ref=xraw.at[source, rows],
+            send_sem=xsend.at[link, c], recv_sem=xrecv.at[source, c],
+            device_id={"sp": target}, device_id_type=MESH,
+        )
+
+    def kv_copy(which, p):
+        hbm, buf, ssem, rsem = ((keys, kraw, ksend, krecv), (values, vb, vsend, vrecv))[which]
+        peer = peers[p]
+        return pltpu.make_async_remote_copy(
+            src_ref=hbm.at[0, :, pl.ds(pl.multiple_of(peer * hd, hd), hd)],
+            dst_ref=buf.at[pl.ds(pl.multiple_of(sp * tokens, tokens), tokens)],
+            send_sem=ssem.at[p], recv_sem=rsem.at[sp],
+            device_id={"sp": peer}, device_id_type=MESH,
+        )
+
+    for h in range(heads):
+        w_send(0, h, start)
+        if h == 0:
+            for c in range(chunks):
+                x_copy(sp, c, 0, across).start()
+                x_copy(sp, c, 1, pair).start()
+    own_x = pltpu.make_async_copy(stream.at[0], xraw.at[sp], own_sem.at[0])
+    own_x.start()
+    own_w = pltpu.make_async_copy(
+        weight.at[:, pl.ds(pl.multiple_of(base, hd), heads * hd)], wb.at[dp], own_sem.at[1]
+    )
+    own_w.start()
+    here = pl.ds(pl.multiple_of(sp * tokens, tokens), tokens)
+    mine = pl.ds(pl.multiple_of(sp * hd, hd), hd)
+    own_k = pltpu.make_async_copy(keys.at[0, :, mine], kraw.at[here], own_sem.at[2])
+    own_v = pltpu.make_async_copy(values.at[0, :, mine], vb.at[here], own_sem.at[3])
+    own_k.start()
+    own_v.start()
+    for p in range(3):
+        kv_copy(0, p).start()
+        kv_copy(1, p).start()
+
+    def norm_rows(source, c):
+        step = 32
+
+        def inner(i, carry):
+            at = pl.multiple_of(c * part + i * step, step)
+            wide = xraw[source, pl.ds(at, step), :].astype(jnp.float32)
+            scale = lax.rsqrt(jnp.mean(wide * wide, axis=-1, keepdims=True) + norm_eps)
+            done = (wide * scale * mix_gain[...]).astype(jnp.bfloat16)
+            to = pl.ds(pl.multiple_of(source * tokens + at, step), step)
+            for d in range(dp_count):
+                xs[d, to, :] = done[:, d * depth : (d + 1) * depth]
+            return carry
+
+        lax.fori_loop(0, part // step, inner, 0)
+
+    def accumulate(block, first=False):
+        tile = 256
+        for n in range(0, heads * hd, tile):
+            term = jnp.dot(xs[block], wb[block, :, n : n + tile], preferred_element_type=jnp.float32)
+            if first:
+                acc[:, n : n + tile] = term
+            else:
+                acc[:, n : n + tile] += term
+
+    own_x.wait()
+    for c in range(chunks):
+        norm_rows(sp, c)
+    for h in range(heads):
+        w_wait(order(1) * nx + x, h)
+        w_send(1, h, start)
+    for c in range(chunks):
+        x_copy(pair, c, 1, pair).wait_recv()
+        norm_rows(pair, c)
+    for rank in range(2, nz - 1):
+        for h in range(heads):
+            w_wait(order(rank) * nx + x, h)
+            w_send(rank, h, start)
+    for c in range(chunks):
+        x_copy(across, c, 0, across).wait_recv()
+        x_copy(across, c, 2, pair).start()
+    for c in range(chunks):
+        norm_rows(across, c)
+
+    own_k.wait()
+    own_v.wait()
+    for p in range(3):
+        rows = pl.ds(pl.multiple_of(peers[p] * tokens, tokens), tokens)
+        for buf, rsem, ssem in ((kraw, krecv, ksend), (vb, vrecv, vsend)):
+            pltpu.make_async_remote_copy(
+                src_ref=buf.at[rows], dst_ref=buf.at[rows], send_sem=ssem.at[p],
+                recv_sem=rsem.at[peers[p]], device_id={"sp": peers[p]}, device_id_type=MESH,
+            ).wait_recv()
+    kn[...] = rms_scaled(kraw[...], key_gain[...])
+
+    for c in range(chunks):
+        x_copy(corner, c, 2, pair).wait_recv()
+        norm_rows(corner, c)
+
+    own_w.wait()
+    accumulate(dp, True)
+    for rank in range(1, nz - 1):
+        accumulate(order(rank) * nx + x)
+    for h in range(heads):
+        w_wait(order(nz - 1) * nx + x, h)
+        w_send(nz - 1, h, start)
+    accumulate(order(nz - 1) * nx + x)
+    for rank in range(nz - 1):
+        block = order(rank) * nx + (1 - x)
+        for h in range(heads):
+            w_wait(block, h)
+        accumulate(block)
+
+    last = order(nz - 1) * nx + (1 - x)
+    size = math.gcd(seq, row_block)
+    rowi = lax.broadcasted_iota(jnp.int32, (size, size), 0)
+    coli = lax.broadcasted_iota(jnp.int32, (size, size), 1)
+    causal = coli < rowi
+    suffix = (rowi >= coli).astype(jnp.float32).astype(jnp.bfloat16)
+
+    def o_copy(h, p, incoming=False):
+        peer = peers[p]
+        owner = peer if incoming else sp
+        return pltpu.make_async_remote_copy(
+            src_ref=ob.at[h, pl.ds(pl.multiple_of(peer * tokens, tokens), tokens)],
+            dst_ref=out.at[0, :, pl.ds(pl.multiple_of(owner * (heads * hd) + h * hd, hd), hd)],
+            send_sem=osend.at[p, h], recv_sem=orecv.at[owner, h],
+            device_id={"sp": peer}, device_id_type=MESH,
+        )
+
+    def o_local(h):
+        return pltpu.make_async_copy(
+            ob.at[h, here],
+            out.at[0, :, pl.ds(pl.multiple_of(base + h * hd, hd), hd)],
+            own_sem.at[4 + h],
+        )
+
+    for h in range(heads):
+        w_wait(last, h)
+        cols = slice(h * hd, (h + 1) * hd)
+        total = acc[:, cols] + jnp.dot(
+            xs[last], wb[last, :, cols], preferred_element_type=jnp.float32
+        )
+        qn = rms_scaled(total.astype(jnp.bfloat16), query_gain[...])
+        off = offset[sp * heads + h]
+        for rb in range(seq // size):
+            q = qn[rb * size : (rb + 1) * size]
+            carry, result = None, None
+            for kb in reversed(range(rb + 1)):
+                at = slice(kb * size, (kb + 1) * size)
+                s = lax.dot_general(
+                    q, kn[at], (((1,), (1,)), ((), ())), preferred_element_type=jnp.float32
+                )
+                s = s * hd ** (-0.5) + off
+                soft = jnp.log(1.0 + jnp.exp(s))
+                if kb == rb:
+                    soft = jnp.where(causal, soft, 0.0)
+                upper = soft.astype(jnp.bfloat16)
+                lower = (soft - upper.astype(jnp.float32)).astype(jnp.bfloat16)
+                sums = jnp.dot(upper, suffix, preferred_element_type=jnp.float32) + jnp.dot(
+                    lower, suffix, preferred_element_type=jnp.float32
+                )
+                if carry is not None:
+                    sums = sums + carry
+                carry = sums[:, 0:1]
+                w = jnp.exp(s - sums)
+                if kb == rb:
+                    w = jnp.where(causal, w, 0.0)
+                term = jnp.dot(w.astype(jnp.bfloat16), vb[at], preferred_element_type=jnp.float32)
+                result = term if result is None else result + term
+            ob[h, rb * size : (rb + 1) * size, :] = result.astype(jnp.bfloat16)
+        for p in (0, 2, 1):
+            o_copy(h, p).start()
+        o_local(h).start()
+
+    for rank in range(nz):
+        for h in range(heads):
+            w_send(rank, h, finish_send)
+    for c in range(chunks):
+        x_copy(sp, c, 0, across).wait_send()
+        x_copy(sp, c, 1, pair).wait_send()
+        x_copy(across, c, 2, pair).wait_send()
+    for p in range(3):
+        kv_copy(0, p).wait_send()
+        kv_copy(1, p).wait_send()
+    for h in range(heads):
+        o_local(h).wait()
+        for p in range(3):
+            o_copy(h, p).wait_send()
+            o_copy(h, p, True).wait_recv()
+
+
+def fused_body(nx, stream, mix_gain, query_weight, query_gain, keys, key_gain, values, stick_offset):
+    sp_count = lax.axis_size("sp")
+    dp_count = lax.axis_size("dp")
+    nz = dp_count // nx
+    tokens, width = stream.shape[1:]
+    depth, columns = query_weight.shape
+    hd = query_gain.shape[0]
+    heads = stick_offset.shape[0] // sp_count
+    seq = tokens * sp_count
+    chunks = 2
+    vmem = pl.BlockSpec(memory_space=pltpu.VMEM)
+    hbm = pl.BlockSpec(memory_space=pl.ANY)
+    dma = pltpu.SemaphoreType.DMA
+    return pl.pallas_call(
+        functools.partial(kernel, nz, nx, heads),
+        out_shape=jax.ShapeDtypeStruct((1, tokens, columns), jnp.bfloat16),
+        in_specs=[hbm, vmem, hbm, vmem, hbm, vmem, hbm, pl.BlockSpec(memory_space=pltpu.SMEM)],
+        out_specs=hbm,
+        scratch_shapes=[
+            pltpu.VMEM((sp_count, tokens, width), jnp.bfloat16),
+            pltpu.VMEM((dp_count, seq, depth), jnp.bfloat16),
+            pltpu.VMEM((dp_count, depth, heads * hd), jnp.bfloat16),
+            pltpu.VMEM((seq, hd), jnp.bfloat16),
+            pltpu.VMEM((seq, hd), jnp.bfloat16),
+            pltpu.VMEM((seq, hd), jnp.bfloat16),
+            pltpu.VMEM((seq, heads * hd), jnp.float32),
+            pltpu.VMEM((heads, seq, hd), jnp.bfloat16),
+            dma((4 + heads,)),
+            dma((dp_count, heads)),
+            dma((3, nz, heads)),
+            dma((sp_count, chunks)),
+            dma((3, chunks)),
+            dma((sp_count,)),
+            dma((3,)),
+            dma((sp_count,)),
+            dma((3,)),
+            dma((sp_count, heads)),
+            dma((3, heads)),
+        ],
+        compiler_params=pltpu.CompilerParams(
+            collective_id=0, has_side_effects=True, vmem_limit_bytes=48 * 1024 * 1024
+        ),
+    )(
+        stream, mix_gain[None], query_weight, query_gain[None], keys, key_gain[None], values,
+        stick_offset,
+    )
+
+
+def widths(mesh):
+    names = tuple(mesh.axis_names)
+    grid = mesh.devices if names == ("dp", "sp") else mesh.devices.T
+    nx = len({d.coords[0] for d in grid[:, 0]})
+    ny = len({d.coords[1] for d in grid[0]})
+    return nx, ny
+
+
 def solution(mesh):
+    nx, ny = widths(mesh)
+    pairs = nx == 2 and ny == 2
+
+    def body(*args):
+        stream, _, _, query_gain, keys = args[:5]
+        sp_count = lax.axis_size("sp")
+        one_head = keys.shape[2] // query_gain.shape[0] == sp_count
+        if pairs and one_head and sp_count == 2 * ny:
+            return fused_body(nx, *args)
+        return general_body(*args)
+
     return jax.shard_map(
         body,
         mesh=mesh,

time: 125 us -> 46.8 us (0.37)
  waiting for transfers between devices: 63.8 us -> 0 us
  Pallas kernels: 0 us -> 41.8 us
  between operations: 13.7 us -> 0.06 us
  matrix products: 13.5 us -> 0 us
  blocking collectives: 11.2 us -> 0 us
  other arithmetic: 9.01 us -> 0 us
  starting transfers between devices: 4.31 us -> 0 us
  local copies, waits for them, and re-layouts: 8.58 us -> 4.75 us
    all_gather x2 -> x0, waiting for transfers between devices: 58.6 us -> none  [the longest x1 37.5 us: body(): gathered = lax.all_gather(columns, 'dp', axis=0, tiled=True)]
    pallas_call x0 -> x1, Pallas kernels: none -> 41.8 us  [fused_body(): pl.pallas_call(functools.partial(kernel, nz, nx, heads), out_shape=jax.Sh...]
    dot_general x7 -> x0, matrix products: 13.5 us -> none  [the longest x2 4.85 us: body(): jnp.einsum('qhd,kd->hqk', mine[first:finish], key_heads[:finish], preferr...]
    all_to_all x1 -> x0, blocking collectives: 11.2 us -> none  [body(): lax.all_to_all(attended, 'sp', split_axis=0, concat_axis=1, tiled=True)]
    convert_element_type x5 -> x0, other arithmetic: 5.95 us -> none  [the longest x3 3.35 us: rms_scaled(): return scaled.astype(jnp.bfloat16)]
    all_to_all x1 -> x0, waiting for transfers between devices: 5.16 us -> none  [body(): lax.all_to_all(copied, 'sp', split_axis=2, concat_axis=0, tiled=True)]
    all_to_all x1 -> x0, starting transfers between devices: 4.26 us -> none  [body(): lax.all_to_all(copied, 'sp', split_axis=2, concat_axis=0, tiled=True)]
    reduce_sum x3 -> x0, other arithmetic: 2.09 us -> none  [rms_scaled(): jnp.mean(wide * wide, axis=-1, keepdims=True) + norm_eps]
  transfers between devices with their start and end apart: 3 -> 0, of which waited for: 3 -> 0; matrix products, arithmetic and copies ran while one was open for 7% -> 0% of each run, Pallas kernels for 0% -> 0%
where the time goes in v1:
time: 46.8 us; the launch traced here: 46.6 us
  Pallas kernels  41.8 us (89%)
  local copies, waits for them, and re-layouts  4.75 us (10%)
    pallas_call x1, Pallas kernels, fused_body(): pl.pallas_call(functools.partial(kernel, nz, nx, heads), out_shape=jax.Sh...  41.8 us
    unnamed x14, local copies, waits for them, and re-layouts  3.94 us

profile of v1, /device:TPU:0, one launch (start us, length us, event | category | flops | bytes accessed | tf_op | source)
XLA Modules:
  0.0 46.6 jit_solution(13159210840383311973)
XLA Ops:
  0.0 0.0 copy-start.5
  0.0 0.0 copy-start.4
  0.0 0.0 copy-start.3
  0.0 0.0 copy-start
  0.0 0.8 %broadcast_in_dim.9.mix_gain = f32[1,2064]{1,0:T(1,128)S(1)} reshape(f32[2064]{0:T(1024)} %param.9) | data formatting | bytes 16512 | tf_op jit(solution)/shard_map/broadcast_in_dim | solution.py:426
  0.8 1.3 %copy.9.stream = bf16[1,128,2064]{2,1,0:T(8,128)(2,1)S(1)} copy(bf16[1,128,2064]{1,2,0:T(8,128)(2,1)} %param.8) | data formatting | bytes 1056768 | tf_op args[0]
  2.1 0.0 copy-done.5
  2.2 0.0 copy-done.4
  2.2 0.0 copy-done.3
  2.2 0.0 copy-done
  2.2 0.0 copy-start.1
  2.2 0.9 %copy-done.1 = bf16[1,128,512]{2,1,0:T(8,128)(2,1)S(1)} copy-done((bf16[1,128,512]{2,1,0:T(8,128)(2,1)S(1)}, bf16[1,128,512]{2,1,0:T(8,128)(2,1)}, u32[]{:S(2)}) %copy-start.1) | copy-done | bytes 131096
  3.1 0.0 copy-start.2
  3.1 0.9 %copy-done.2 = bf16[1,128,512]{2,1,0:T(8,128)(2,1)S(1)} copy-done((bf16[1,128,512]{2,1,0:T(8,128)(2,1)S(1)}, bf16[1,128,512]{2,1,0:T(8,128)(2,1)}, u32[]{:S(2)}) %copy-start.2) | copy-done | bytes 131096
  4.0 41.8 %shard_map.82 = bf16[1,128,2048]{2,1,0:T(8,128)(2,1)S(1)} custom-call(bf16[1,128,2064]{2,1,0:T(8,128)(2,1)S(1)} %copy.9.stream, f32[1,2064]{1,0:T(1,128)S(1)} %broadcast_in_dim.9.mix_gain, bf16[258,2048]{1,0:T(8,128)(2,1)S(1)} %copy-done, f32[1,128]{1,0:T(1,128)S(1)} %bitcast.2, bf16[1,128,512]{2,1,0:T(8,128)(2,1)S(1)} %copy-done.1, f32[1,128]{1,0:T(1,128)S(1)} %bitcast.3, ...), custom_call_target="tpu_custom_call" | custom-call | tf_op jit(solution)/shard_map/pallas_call | solution.py:396
  45.8 0.8 %copy.11 = bf16[1,128,2048]{2,1,0:T(8,128)(2,1)} copy(bf16[1,128,2048]{2,1,0:T(8,128)(2,1)S(1)} %shard_map.82) | data formatting | bytes 1048576
Async XLA Ops:
  0.0 2.1 %copy-start.5 = (f32[16]{0:T(128)S(1)}, f32[16]{0:T(128)}, u32[]{:S(2)}) copy-start(f32[16]{0:T(128)} %offset.1) | copy-start | bytes 196
  0.0 2.2 %copy-start.4 = (f32[128]{0:T(128)S(1)}, f32[128]{0:T(128)}, u32[]{:S(2)}) copy-start(f32[128]{0:T(128)} %param.13) | copy-start | bytes 1540
  0.0 2.2 %copy-start.3 = (f32[128]{0:T(128)S(1)}, f32[128]{0:T(128)}, u32[]{:S(2)}) copy-start(f32[128]{0:T(128)} %param.11) | copy-start | bytes 1540
  0.0 2.2 %copy-start = (bf16[258,2048]{1,0:T(8,128)(2,1)S(1)}, bf16[258,2048]{1,0:T(8,128)(2,1)}, u32[]{:S(2)}) copy-start(bf16[258,2048]{1,0:T(8,128)(2,1)} %weight.1) | copy-start | bytes 3170308
  2.2 0.9 %copy-start.1 = (bf16[1,128,512]{2,1,0:T(8,128)(2,1)S(1)}, bf16[1,128,512]{2,1,0:T(8,128)(2,1)}, u32[]{:S(2)}) copy-start(bf16[1,128,512]{2,1,0:T(8,128)(2,1)} %keys.1) | copy-start | bytes 393220
  3.1 0.9 %copy-start.2 = (bf16[1,128,512]{2,1,0:T(8,128)(2,1)S(1)}, bf16[1,128,512]{2,1,0:T(8,128)(2,1)}, u32[]{:S(2)}) copy-start(bf16[1,128,512]{2,1,0:T(8,128)(2,1)} %values.1) | copy-start | bytes 393220

commit v2 on v1

--- a/solution.py
+++ b/solution.py
@@ -100,12 +100,12 @@
 def kernel(
     nz, nx, heads, stream, mix_gain, weight, query_gain, keys, key_gain, values, offset, out,
     xraw, xs, wb, kraw, kn, vb, acc, ob,
-    own_sem, wrecv, wsend, xrecv, xsend, krecv, ksend, vrecv, vsend, orecv, osend,
+    own_sem, wrecv, zsend, wsend, fsend, xrecv, xsend, krecv, ksend, vrecv, vsend, orecv, osend,
 ):
     sp_count = xraw.shape[0]
     tokens, width = xraw.shape[1:]
     seq = sp_count * tokens
-    hd = query_gain.shape[1]
+    hd = query_gain.shape[0]
     depth = wb.shape[1]
     dp_count = nz * nx
     dp = lax.axis_index("dp")
@@ -139,46 +139,90 @@
     low, high = z, nz - 1 - z
     both = jnp.minimum(low, high)
 
+    upper_half = low > high
+
     def order(i):
         if i == 0:
             return z
-        near = z + (i + 1) // 2 if i % 2 else z - i // 2
-        far = jnp.where(high > low, z + (i - both), z - (i - both))
+        step = (i + 1) // 2 if i % 2 else -(i // 2)
+        near = jnp.where(upper_half, z + step, z - step)
+        far = jnp.where(upper_half, z - (i - both), z + (i - both))
         return jnp.where(i <= 2 * both, near, far)
 
-    def w_copy(link, target, rank, h):
-        zz = order(rank)
-        block = zz * nx + x
-        if rank == 0:
-            src = weight.at[:, pl.ds(pl.multiple_of(base + h * hd, hd), hd)]
+    def w_copy(block, h, sem, target, own=False):
+        ref = wb.at[block, :, pl.ds(h * hd, hd)]
+        src = weight.at[:, pl.ds(pl.multiple_of(base + h * hd, hd), hd)] if own else ref
+        return pltpu.make_async_remote_copy(
+            src_ref=src, dst_ref=ref, send_sem=sem, recv_sem=wrecv.at[block, h],
+            device_id={"dp": target}, device_id_type=MESH,
+        )
+
+    def z_send(k, h, act):
+        @pl.when((z + k < nz) & has_down)
+        def _():
+            act(w_copy((z + k) * nx + x, h, zsend.at[0, k, h], dp - nx, k == 0))
+
+        @pl.when((z - k >= 0) & has_up)
+        def _():
+            act(w_copy((z - k) * nx + x, h, zsend.at[1, k, h], dp + nx, k == 0))
+
+    def z_step(k, h):
+        @pl.when(z + k < nz)
+        def _():
+            w_wait((z + k) * nx + x, h)
+
+        @pl.when(z - k >= 0)
+        def _():
+            w_wait((z - k) * nx + x, h)
+
+        z_send(k, h, start)
+
+    def side_send(rank, h, act):
+        if rank < nz - 1 or h % 2 == 0:
+            act(w_copy(order(rank) * nx + x, h, wsend.at[rank, h], side, rank == 0))
+
+    inner = both == nz // 2 - 1
+    inward = jnp.where(upper_half, dp - nx, dp + nx)
+    outward = jnp.where(upper_half, dp + nx, dp - nx)
+    edge = jnp.where(upper_half, nz - 1, 0) * nx + (1 - x)
+    opposite = jnp.where(upper_half, 0, nz - 1) * nx + (1 - x)
+
+    def far_in(h, act):
+        @pl.when(inner)
+        def _():
+            act(w_copy(edge, h, fsend.at[0, h], inward))
+
+    def far_out(h, act):
+        @pl.when(both > 0)
+        def _():
+            act(w_copy(opposite, h, fsend.at[1, h], outward))
+
+    def far_in_step(h):
+        @pl.when(inner)
+        def _():
+            w_wait(edge, h)
+
+        far_in(h, start)
+
+    def far_out_step(h):
+        w_wait(opposite, h)
+        far_out(h, start)
+
+    def side_wait(rank, h):
+        if rank == nz - 1 and h % 2:
+            return
+        if rank == nz - 3 and h % 2:
+
+            @pl.when(jnp.logical_not(inner))
+            def _():
+                w_wait(order(rank) * nx + (1 - x), h)
         else:
-            src = wb.at[block, :, pl.ds(h * hd, hd)]
-        return pltpu.make_async_remote_copy(
-            src_ref=src,
-            dst_ref=wb.at[block, :, pl.ds(h * hd, hd)],
-            send_sem=wsend.at[link, rank, h],
-            recv_sem=wrecv.at[block, h],
-            device_id={"dp": target},
-            device_id_type=MESH,
-        )
-
-    def w_send(rank, h, act):
-        zz = order(rank)
-
-        @pl.when(has_up & (zz <= z))
-        def _():
-            act(w_copy(0, dp + nx, rank, h))
-
-        @pl.when(has_down & (zz >= z))
-        def _():
-            act(w_copy(1, dp - nx, rank, h))
-
-        act(w_copy(2, side, rank, h))
+            w_wait(order(rank) * nx + (1 - x), h)
 
     def w_wait(block, h):
         ref = wb.at[block, :, pl.ds(h * hd, hd)]
         pltpu.make_async_remote_copy(
-            src_ref=ref, dst_ref=ref, send_sem=wsend.at[0, 0, 0], recv_sem=wrecv.at[block, h],
+            src_ref=ref, dst_ref=ref, send_sem=wsend.at[0, 0], recv_sem=wrecv.at[block, h],
             device_id={"dp": side}, device_id_type=MESH,
         ).wait_recv()
 
@@ -207,12 +251,16 @@
             device_id={"sp": peer}, device_id_type=MESH,
         )
 
-    for h in range(heads):
-        w_send(0, h, start)
-        if h == 0:
-            for c in range(chunks):
-                x_copy(sp, c, 0, across).start()
-                x_copy(sp, c, 1, pair).start()
+    def both_send(k, h):
+        z_send(k, h, start)
+        side_send(k, h, start)
+
+    both_send(0, 0)
+    for c in range(chunks):
+        x_copy(sp, c, 0, across).start()
+        x_copy(sp, c, 1, pair).start()
+    for h in range(1, heads - 1):
+        both_send(0, h)
     own_x = pltpu.make_async_copy(stream.at[0], xraw.at[sp], own_sem.at[0])
     own_x.start()
     own_w = pltpu.make_async_copy(
@@ -231,12 +279,13 @@
 
     def norm_rows(source, c):
         step = 32
+        gain = mix_gain[...].reshape(1, width)
 
         def inner(i, carry):
             at = pl.multiple_of(c * part + i * step, step)
             wide = xraw[source, pl.ds(at, step), :].astype(jnp.float32)
             scale = lax.rsqrt(jnp.mean(wide * wide, axis=-1, keepdims=True) + norm_eps)
-            done = (wide * scale * mix_gain[...]).astype(jnp.bfloat16)
+            done = (wide * scale * gain).astype(jnp.bfloat16)
             to = pl.ds(pl.multiple_of(source * tokens + at, step), step)
             for d in range(dp_count):
                 xs[d, to, :] = done[:, d * depth : (d + 1) * depth]
@@ -256,52 +305,65 @@
     own_x.wait()
     for c in range(chunks):
         norm_rows(sp, c)
-    for h in range(heads):
-        w_wait(order(1) * nx + x, h)
-        w_send(1, h, start)
-    for c in range(chunks):
-        x_copy(pair, c, 1, pair).wait_recv()
-        norm_rows(pair, c)
-    for rank in range(2, nz - 1):
-        for h in range(heads):
-            w_wait(order(rank) * nx + x, h)
-            w_send(rank, h, start)
-    for c in range(chunks):
+
+    def pair_rows():
+        for c in range(chunks):
+            x_copy(pair, c, 1, pair).wait_recv()
+            norm_rows(pair, c)
+
+    def across_in(c):
         x_copy(across, c, 0, across).wait_recv()
         x_copy(across, c, 2, pair).start()
-    for c in range(chunks):
-        norm_rows(across, c)
-
-    own_k.wait()
-    own_v.wait()
-    for p in range(3):
-        rows = pl.ds(pl.multiple_of(peers[p] * tokens, tokens), tokens)
-        for buf, rsem, ssem in ((kraw, krecv, ksend), (vb, vrecv, vsend)):
-            pltpu.make_async_remote_copy(
-                src_ref=buf.at[rows], dst_ref=buf.at[rows], send_sem=ssem.at[p],
-                recv_sem=rsem.at[peers[p]], device_id={"sp": peers[p]}, device_id_type=MESH,
-            ).wait_recv()
-    kn[...] = rms_scaled(kraw[...], key_gain[...])
-
-    for c in range(chunks):
-        x_copy(corner, c, 2, pair).wait_recv()
-        norm_rows(corner, c)
-
+
+    def key_rows():
+        own_k.wait()
+        own_v.wait()
+        for p in range(3):
+            rows = pl.ds(pl.multiple_of(peers[p] * tokens, tokens), tokens)
+            for buf, rsem, ssem in ((kraw, krecv, ksend), (vb, vrecv, vsend)):
+                pltpu.make_async_remote_copy(
+                    src_ref=buf.at[rows], dst_ref=buf.at[rows], send_sem=ssem.at[p],
+                    recv_sem=rsem.at[peers[p]], device_id={"sp": peers[p]}, device_id_type=MESH,
+                ).wait_recv()
+        kn[...] = rms_scaled(kraw[...], key_gain[...].reshape(1, hd))
+
+    steps = []
+    for k in range(1, nz):
+        for h in range(heads):
+            steps.append((2 * k + h, -k, functools.partial(z_step, k, h)))
+            steps.append((2 * k + h, -k, functools.partial(side_send, k, h, start)))
+    steps.append((heads - 1, 0, functools.partial(both_send, 0, heads - 1)))
+    for h in range(1, heads, 2):
+        steps.append((2 * nz - 4 + h + 0.5, -nz, functools.partial(far_in_step, h)))
+        steps.append((2 * nz - 1 + h, -nz, functools.partial(far_out_step, h)))
+    steps.sort(key=lambda step: step[:2])
+
+    def advance(limit):
+        while steps and steps[0][0] <= limit:
+            steps.pop(0)[2]()
+
+    advance(3)
+    pair_rows()
+    advance(4)
+    across_in(0)
+    advance(6)
+    norm_rows(across, 0)
+    advance(7)
+    across_in(1)
+    norm_rows(across, 1)
+    x_copy(corner, 0, 2, pair).wait_recv()
+    norm_rows(corner, 0)
+    advance(8)
+    x_copy(corner, 1, 2, pair).wait_recv()
+    norm_rows(corner, 1)
     own_w.wait()
     accumulate(dp, True)
-    for rank in range(1, nz - 1):
-        accumulate(order(rank) * nx + x)
     for h in range(heads):
-        w_wait(order(nz - 1) * nx + x, h)
-        w_send(nz - 1, h, start)
-    accumulate(order(nz - 1) * nx + x)
-    for rank in range(nz - 1):
-        block = order(rank) * nx + (1 - x)
-        for h in range(heads):
-            w_wait(block, h)
-        accumulate(block)
-
-    last = order(nz - 1) * nx + (1 - x)
+        side_wait(0, h)
+    accumulate(side)
+    accumulate(order(1) * nx + x)
+    key_rows()
+
     size = math.gcd(seq, row_block)
     rowi = lax.broadcasted_iota(jnp.int32, (size, size), 0)
     coli = lax.broadcasted_iota(jnp.int32, (size, size), 1)
@@ -326,12 +388,18 @@
         )
 
     for h in range(heads):
-        w_wait(last, h)
+        advance(2 * nz + h if h else 2 * nz)
         cols = slice(h * hd, (h + 1) * hd)
-        total = acc[:, cols] + jnp.dot(
-            xs[last], wb[last, :, cols], preferred_element_type=jnp.float32
-        )
-        qn = rms_scaled(total.astype(jnp.bfloat16), query_gain[...])
+        total = acc[:, cols]
+        blocks = [order(rank) * nx + x for rank in range(2, nz)]
+        for rank in range(1, nz):
+            side_wait(rank, h)
+            blocks.append(order(rank) * nx + (1 - x))
+        for block in blocks:
+            total = total + jnp.dot(
+                xs[block], wb[block, :, cols], preferred_element_type=jnp.float32
+            )
+        qn = rms_scaled(total.astype(jnp.bfloat16), query_gain[...].reshape(1, hd))
         off = offset[sp * heads + h]
         for rb in range(seq // size):
             q = qn[rb * size : (rb + 1) * size]
@@ -363,9 +431,13 @@
             o_copy(h, p).start()
         o_local(h).start()
 
-    for rank in range(nz):
-        for h in range(heads):
-            w_send(rank, h, finish_send)
+    for h in range(heads):
+        for k in range(nz):
+            z_send(k, h, finish_send)
+            side_send(k, h, finish_send)
+        if h % 2:
+            far_in(h, finish_send)
+            far_out(h, finish_send)
     for c in range(chunks):
         x_copy(sp, c, 0, across).wait_send()
         x_copy(sp, c, 1, pair).wait_send()
@@ -409,7 +481,9 @@
             pltpu.VMEM((heads, seq, hd), jnp.bfloat16),
             dma((4 + heads,)),
             dma((dp_count, heads)),
-            dma((3, nz, heads)),
+            dma((2, nz, heads)),
+            dma((nz, heads)),
+            dma((2, heads)),
             dma((sp_count, chunks)),
             dma((3, chunks)),
             dma((sp_count,)),
@@ -420,10 +494,10 @@
             dma((3, heads)),
         ],
         compiler_params=pltpu.CompilerParams(
-            collective_id=0, has_side_effects=True, vmem_limit_bytes=48 * 1024 * 1024
+            collective_id=0, has_side_effects=True, vmem_limit_bytes=62 * 1024 * 1024
         ),
     )(
-        stream, mix_gain[None], query_weight, query_gain[None], keys, key_gain[None], values,
+        stream, mix_gain, query_weight, query_gain, keys, key_gain, values,
         stick_offset,
     )
 
@@ -444,7 +518,8 @@
         stream, _, _, query_gain, keys = args[:5]
         sp_count = lax.axis_size("sp")
         one_head = keys.shape[2] // query_gain.shape[0] == sp_count
-        if pairs and one_head and sp_count == 2 * ny:
+        nz = lax.axis_size("dp") // nx
+        if pairs and one_head and sp_count == 2 * ny and nz >= 4 and nz % 2 == 0:
             return fused_body(nx, *args)
         return general_body(*args)
 

time: 46.8 us -> 43.8 us (0.936)
  Pallas kernels: 41.8 us -> 39.6 us
  local copies, waits for them, and re-layouts: 4.75 us -> 3.95 us
    pallas_call x1, Pallas kernels: 41.8 us -> 39.6 us  [fused_body(): pl.pallas_call(functools.partial(kernel, nz, nx, heads), out_shape=jax.Sh...]
    broadcast_in_dim x1 -> x0, local copies, waits for them, and re-layouts: 0.8 us -> none  [fused_body(): mix_gain[None]]
    unnamed x14 -> x2, local copies, waits for them, and re-layouts: 3.94 us -> 3.95 us
where the time goes in v2:
time: 43.8 us; the launch traced here: 43.6 us
  Pallas kernels  39.6 us (90%)
  local copies, waits for them, and re-layouts  3.95 us (9%)
    pallas_call x1, Pallas kernels, fused_body(): pl.pallas_call(functools.partial(kernel, nz, nx, heads), out_shape=jax.Sh...  39.6 us
    unnamed x2, local copies, waits for them, and re-layouts  3.95 us

profile of v2, /device:TPU:0, one launch (start us, length us, event | category | flops | bytes accessed | tf_op | source)
XLA Modules:
  0.0 43.6 jit_solution(18127773771411090941)
XLA Ops:
  0.0 2.1 %copy.9.stream = bf16[1,128,2064]{2,1,0:T(8,128)(2,1)} copy(bf16[1,128,2064]{1,2,0:T(8,128)(2,1)} %param.8) | data formatting | bytes 1056768 | tf_op args[0]
  2.1 39.6 %shard_map.82 = bf16[1,128,2048]{2,1,0:T(8,128)(2,1)} custom-call(bf16[1,128,2064]{2,1,0:T(8,128)(2,1)} %copy.9.stream, f32[2064]{0:T(1024)} %mix_gain.1, bf16[258,2048]{1,0:T(8,128)(2,1)} %weight.1, f32[128]{0:T(128)} %query_gain.1, bf16[1,128,512]{2,1,0:T(8,128)(2,1)} %keys.1, f32[128]{0:T(128)} %key_gain.1, bf16[1,128,512]{2,1,0:T(8,128)(2,1)} %values.1, ...), custom_call_target="tpu_custom_call" | custom-call | tf_op jit(solution)/shard_map/pallas_call | solution.py:468
  41.7 1.9 %copy.11 = bf16[1,128,2048]{2,1,0:T(8,128)(2,1)} copy(bf16[1,128,2048]{2,1,0:T(8,128)(2,1)} %shard_map.82) | data formatting | bytes 1048576
